TPU v7x, 256 devices: a whole 4x4x8 slice. The times are simulated.
256 devices in a mesh: sp: 32 (over z, x), tp: 8 (over y, core).
Axes of the slice: x: 4, y: 4, z: 8, core: 2. Of those that a mesh axis runs over, the one named last changes fastest.
Arguments:
- residual: bfloat16 [24576, 2048], P('sp'), may hold values from -6 to 6
- queries: bfloat16 [24576, 1024], P('sp', 'tp'), may hold values from -12 to 12
- keys: bfloat16 [24576, 512], P('sp', 'tp'), may hold values from -6 to 6
- values: bfloat16 [24576, 512], P('sp', 'tp'), may hold values from -36 to 36
- segments: int32 [24576], P('sp'), may hold values from 0 to 15, never falling along the last dimension, each value on 1 to 3072 neighbouring positions
- sink: float32 [16], P('tp'), may hold values from 3 to 7
- out_weight: bfloat16 [1024, 2048], replicated, may hold values from -0.1875 to 0.1875
- norm_gain_one: float32 [2048], replicated, may hold values from 0.1 to 1.9
- group: int32 [24576], P('sp'), may hold values from 0 to 3, as said below
- member: int32 [24576, 2], P('sp'), may hold values from 0 to 7, as said below
- route_weight: float32 [24576, 2], P('sp'), may hold values from 0.25 to 1
- gate_weight: bfloat16 [32, 2048, 1024], P('sp', None, 'tp'), may hold values from -0.125 to 0.125
- up_weight: bfloat16 [32, 2048, 1024], P('sp', None, 'tp'), may hold values from -0.125 to 0.125
- down_weight: bfloat16 [32, 1024, 2048], P('sp', None, 'tp'), may hold values from -0.1875 to 0.1875
- norm_gain_two: float32 [2048], P('tp'), may hold values from 0.1 to 1.9
Outputs:
- output: bfloat16 [24576, 2048], P('sp', 'tp')
Inputs may be any that keep to these rules, and one draw needn't show every extreme that they name: In every aligned block of 96 rows no expert (group * 8 + member) is named by more than 12 rows, and one expert, the same in all blocks of a draw, is named by exactly 12 rows of every block. `member`: the 2 members of a row differ.
All inputs are finite; a program needn't handle non-finite values.
Results may differ from a plain program's by a relative error of at most 0.0059.
Values may be sent and summed in bfloat16 or wider, within the bound.
No kernel may reach another device: no remote copies, remote signals or barrier semaphores. Data moves between devices by JAX's collectives and lax.ppermute only.
A program may use at most 128 MiB of HBM per device.

v0:
```python
import math

import jax
import jax.numpy as jnp
from jax import lax
from jax.sharding import PartitionSpec as P

HEAD_DIM = 64
HALF = 128
PER_GROUP = 8


ALPHA = 2.0**0.25
EPS = 1e-05


def with_halo(block, sides, width):
    for axis, dim in sides:
        count = lax.axis_size(axis)
        forward = [(i, i + 1) for i in range(count - 1)]
        backward = [(target, source) for source, target in forward]
        low = lax.ppermute(
            lax.slice_in_dim(block, block.shape[dim] - width, None, axis=dim), axis, forward
        )
        high = lax.ppermute(lax.slice_in_dim(block, 0, width, axis=dim), axis, backward)
        block = jnp.concatenate([low, block, high], axis=dim)
    return block


def copy_for_each(x, axis):
    copies = jnp.broadcast_to(x, (lax.axis_size(axis), *x.shape))
    return lax.all_to_all(copies, axis, split_axis=0, concat_axis=0, tiled=True)


def joined_along(pieces, dim):
    pieces = jnp.moveaxis(pieces, 0, dim)
    lengths = pieces.shape
    return pieces.reshape(*lengths[:dim], lengths[dim] * lengths[dim + 1], *lengths[dim + 2 :])


def gather_directly(x, axis, dim):
    pieces = copy_for_each(x, axis)
    return joined_along(pieces, dim)


def taken_together(x, axis):
    everything = copy_for_each(x, axis)
    return jnp.sum(everything, axis=0)


def packed_total(arrays, axis):
    ends = [0]
    for a in arrays:
        ends.append(ends[-1] + a.size)
    subtotal = taken_together(jnp.concatenate([a.ravel() for a in arrays]), axis)
    return tuple((subtotal[b:e].reshape(a.shape) for a, b, e in zip(arrays, ends, ends[1:])))


def layer_norm(summed, norm_gain):
    mean_value = jnp.mean(summed, -1, keepdims=True)
    variance = jnp.mean(jnp.square(summed - mean_value), -1, keepdims=True)
    return ((summed - mean_value) * lax.rsqrt(variance + EPS) * norm_gain).astype(jnp.bfloat16)


def shards(
    residual,
    queries,
    keys,
    values,
    segments,
    sink,
    out_weight,
    norm_gain_one,
    group,
    member,
    route_weight,
    gate_weight,
    up_weight,
    down_weight,
    norm_gain_two,
):
    row_count = queries.shape[0]
    sp_size = lax.axis_size("sp")
    tp_size = lax.axis_size("tp")
    kv_local = keys.shape[1] // HEAD_DIM
    heads_local = queries.shape[1] // HEAD_DIM
    group_size = heads_local // kv_local
    seq_total = row_count * sp_size
    seq_start = lax.axis_index("sp") * row_count
    joined = jnp.concatenate([keys, values], axis=1)
    padded, seg_padded = (
        with_halo(joined, (("sp", 0),), HALF),
        with_halo(segments, (("sp", 0),), HALF),
    )
    query_block = math.gcd(row_count, 512)
    key_span = query_block + 2 * HALF
    offsets = jnp.arange(key_span)[None, :] - HALF - jnp.arange(query_block)[:, None]
    in_band = jnp.abs(offsets) <= HALF
    sink_heads = sink.reshape(kv_local, group_size, 1, 1)
    query_heads = queries.reshape(row_count, kv_local, group_size, HEAD_DIM)
    key_cols = kv_local * HEAD_DIM
    pieces = []
    for number in range(row_count // query_block):
        row_low = number * query_block
        query_rows = query_heads[row_low : row_low + query_block]
        kv_rows = padded[row_low : row_low + key_span]
        key_part = kv_rows[:, :key_cols].reshape(key_span, kv_local, HEAD_DIM)
        value_part = kv_rows[:, key_cols:].reshape(key_span, kv_local, HEAD_DIM)
        key_place = seq_start + row_low - HALF + jnp.arange(key_span)
        inside = (key_place >= 0) & (key_place < seq_total)
        same_doc = (
            segments[row_low : row_low + query_block, None]
            == seg_padded[None, row_low : row_low + key_span]
        )
        allowed = in_band & same_doc & inside[None, :]
        scores = jnp.einsum(
            "qkgd,ckd->kgqc", query_rows, key_part, preferred_element_type=jnp.float32
        ) * HEAD_DIM ** (-0.5)
        masked = jnp.where(allowed, scores, -1e30)
        peak = jnp.maximum(jnp.max(masked, -1, keepdims=True), sink_heads)
        raised = jnp.where(allowed, jnp.exp(masked - peak), 0.0)
        denominator = jnp.sum(raised, -1, keepdims=True) + jnp.exp(sink_heads - peak)
        weights = (raised / denominator).astype(jnp.bfloat16)
        attended_part = jnp.einsum(
            "kgqc,ckd->qkgd", weights, value_part, preferred_element_type=jnp.float32
        )
        pieces.append(
            attended_part.reshape(query_block, heads_local * HEAD_DIM).astype(jnp.bfloat16)
        )
    attended = jnp.concatenate(pieces, 0)
    width = out_weight.shape[1]
    weight_rows = out_weight
    mixed = jnp.dot(
        gather_directly(attended, "tp", 1), weight_rows, preferred_element_type=jnp.float32
    )
    pre_one = ALPHA * residual.astype(jnp.float32) + mixed
    normed = layer_norm(pre_one, norm_gain_one)
    experts_local = gate_weight.shape[0]
    expert_count = experts_local * sp_size
    picks_count = member.shape[1]
    block_rows = row_count // tp_size
    capacity = max(2, block_rows // 8)
    expert_ids = (group[:, None] * PER_GROUP + member).reshape(tp_size, block_rows * picks_count)
    onehot_table = (expert_ids[:, :, None] == jnp.arange(expert_count)[None, None, :]).astype(
        jnp.int32
    )
    ranks = jnp.sum((jnp.cumsum(onehot_table, 1) - 1) * onehot_table, 2)
    owner = expert_ids // experts_local
    local_ids = expert_ids % experts_local
    block_ids = jnp.arange(tp_size)[:, None]
    slot_all = ((local_ids * sp_size + owner) * tp_size + block_ids) * capacity + ranks
    copy_rows = (
        jnp.arange(row_count * picks_count).reshape(tp_size, block_rows * picks_count)
        // picks_count
    )
    extended = jnp.concatenate([normed, jnp.zeros((1, width), jnp.bfloat16)], 0)
    tp_place = lax.axis_index("tp")
    slot_own_base = (local_ids * sp_size + owner) * capacity + ranks
    own_slots = lax.dynamic_index_in_dim(slot_own_base, tp_place, 0, keepdims=False)
    own_rows = lax.dynamic_index_in_dim(copy_rows, tp_place, 0, keepdims=False)
    slot_count = experts_local * sp_size * capacity
    source = jnp.full((slot_count,), row_count, jnp.int32).at[own_slots].set(own_rows)
    outgoing = extended[source].reshape(experts_local, sp_size, capacity, width)
    received = lax.all_to_all(outgoing, "sp", split_axis=1, concat_axis=1, tiled=True)
    arrived = lax.all_gather(received, "tp", axis=2, tiled=True)
    expert_rows = arrived.reshape(experts_local, sp_size * tp_size * capacity, width)
    gate_part = jnp.einsum(
        "esd,edf->esf", expert_rows, gate_weight, preferred_element_type=jnp.float32
    )
    up_part = jnp.einsum("esd,edf->esf", expert_rows, up_weight, preferred_element_type=jnp.float32)
    hidden = (jax.nn.silu(gate_part) * up_part).astype(jnp.bfloat16)
    column_width = down_weight.shape[2]
    weight_rows = down_weight
    produced = jnp.einsum(
        "esf,efc->esc",
        lax.all_gather(hidden, "tp", axis=2, tiled=True),
        weight_rows,
        preferred_element_type=jnp.float32,
    ).astype(jnp.bfloat16)
    returned = lax.all_to_all(
        produced.reshape(experts_local, sp_size, tp_size * capacity, column_width),
        "sp",
        split_axis=1,
        concat_axis=1,
        tiled=True,
    )
    result_rows = returned.reshape(-1, column_width)
    picked = result_rows[slot_all.reshape(row_count, picks_count)]
    combined = jnp.sum(route_weight[:, :, None] * picked.astype(jnp.float32), 1)
    column_start = lax.axis_index("tp") * column_width
    normed_part = lax.dynamic_slice_in_dim(normed, column_start, column_width, 1)
    pre_two = ALPHA * normed_part.astype(jnp.float32) + combined
    sums, squares = packed_total((jnp.sum(pre_two, -1), jnp.sum(pre_two * pre_two, -1)), "tp")
    mean_value = (sums / width)[:, None]
    variance = (squares / width)[:, None] - mean_value * mean_value
    return ((pre_two - mean_value) * lax.rsqrt(variance + EPS) * norm_gain_two).astype(jnp.bfloat16)


def solution(mesh):
    in_specs = (
        P("sp", None),
        P("sp", "tp"),
        P("sp", "tp"),
        P("sp", "tp"),
        P("sp"),
        P("tp"),
        P(),
        P(),
        P("sp"),
        P("sp", None),
        P("sp", None),
        P("sp", None, "tp"),
        P("sp", None, "tp"),
        P("sp", None, "tp"),
        P("tp"),
    )
    out_specs = P("sp", "tp")
    return jax.shard_map(shards, mesh=mesh, in_specs=in_specs, out_specs=out_specs, check_vma=False)
```

profile of v0, /device:TPU:1, one launch (start us, length us, event | category | flops | bytes accessed | tf_op | source)
XLA Modules:
  0.0 366.8 jit_solution(6680165087132534622)
XLA Ops:
  6.5 0.8 fusion.64
  7.4 3.9 %collective-permute-start.1 = (s32[128]{0:T(128)S(1)}, s32[128]{0:T(128)S(1)}, u32[]{:S(2)}, u32[]{:S(2)}) collective-permute-start(s32[128]{0:T(128)S(1)} %get-tuple-element.16), channel_id=1, source_target_pairs={{0,8},{8,16},{16,24},{24,32},{32,40},{40,48},{48,56},{56,64},{64,7... | collective-permute-start | bytes 1544 | tf_op jit(solution)/shard_map/ppermute | solution.py:22
  11.3 1.3 collective-permute-start.3
  12.6 0.9 constant_dynamic-update-slice_fusion.1
  13.5 0.9 constant_dynamic-update-slice_fusion
  14.4 4.0 %collective-permute-start = (bf16[128,128]{0,1:T(8,128)(2,1)S(1)}, bf16[128,128]{0,1:T(8,128)(2,1)S(1)}, u32[]{:S(2)}, u32[]{:S(2)}) collective-permute-start(bf16[128,128]{0,1:T(8,128)(2,1)S(1)} %get-tuple-element.7), channel_id=1, source_target_pairs={{0,8},{8,16},{16,24},{24,32},{32,40},{40,48},{48,56},{56,64},{64,7... | collective-permute-start | bytes 98312 | tf_op jit(solution)/shard_map/ppermute | solution.py:22
  18.4 1.3 collective-permute-start.2
  19.7 0.8 fusion.65
  20.5 0.7 broadcast_multiply_fusion
  21.2 0.9 fusion.63
  22.1 0.9 copy.90
  23.0 0.2 broadcast_add_fusion
  23.2 0.2 reshape.414
  23.5 0.7 slice.98
  24.2 0.1 copy.83
  24.3 0.1 copy.87
  24.4 0.1 copy.85
  24.6 0.7 and_and_fusion.2
  25.4 0.3 fusion.67
  25.7 0.3 fusion.66
  26.1 0.2 fusion.7
  26.4 0.3 fusion.68
  26.8 0.2 fusion.8
  27.0 0.2 fusion.9
  27.2 0.1 exponential_add_fusion.1
  27.3 0.4 convolution_convert_fusion.1
  27.7 0.4 convolution_convert_fusion.3
  28.1 0.4 convolution_convert_fusion.2
  28.5 1.3 broadcast_in_dim.73
  29.7 6.0 %all-to-all-start = ((bf16[8,768,128]{1,2,0:T(8,128)(2,1)}), bf16[8,768,128]{1,2,0:T(8,128)(2,1)S(1)}, u32[]{:S(2)}, u32[]{:S(2)}) async-start(bf16[8,768,128]{1,2,0:T(8,128)(2,1)} %broadcast_in_dim.73), calls=%async_computation | async-start | bytes 3145728 | tf_op jit(solution)/shard_map/all_to_all | solution.py:32
  35.7 4.6 %reduce-window.6 = s32[8,32,2,128]{3,1,2,0:T(8,128)S(1)} reduce-window(s32[8,32,2,128]{3,1,2,0:T(8,128)S(1)} %copy_bitcast_fusion, s32[]{:T(128)} %constant.104.clone.1), window={size=1x1x1x128 pad=0_0x0_0x0_0x127_0}, to_apply=%region_8.9 | reduce-window | flops 8323072 | bytes 524292 | tf_op jit(solution)/shard_map/reduce-window
  40.4 0.1 slice.120
  40.5 0.2 copy.92
  40.7 0.1 bitcast_bitcast_fusion
  41.0 1.4 scatter_custom_fusion
  42.4 13.9 %all-to-all-done = bf16[8,768,128]{1,2,0:T(8,128)(2,1)S(1)} async-done(((bf16[8,768,128]{1,2,0:T(8,128)(2,1)}), bf16[8,768,128]{1,2,0:T(8,128)(2,1)S(1)}, u32[]{:S(2)}, u32[]{:S(2)}) %all-to-all-start) | async-done | bytes 1572896 | tf_op jit(solution)/shard_map/all_to_all | solution.py:32
  56.3 7.3 %fusion.69 = (f32[768]{0:T(1024)S(1)}, f32[768,2048]{1,0:T(8,128)S(1)}) fusion(bf16[768,1024]{0,1:T(8,128)(2,1)S(1)} %bitcast.123, bf16[1024,2048]{1,0:T(8,128)(2,1)} %param.21, bf16[768,2048]{1,0:T(8,128)(2,1)} %param.15), kind=kOutput, calls=%fused_computation.143 | convolution fusion | flops 3227516160 | bytes 15207424 | tf_op jit(solution)/shard_map/dot_general | solution.py:133
  63.7 0.8 multiply_reduce_fusion
  64.5 0.9 multiply_convert_fusion
  65.4 1.7 copy-done.1
  67.0 2.0 concatenate.32
  69.1 7.4 %gather_fusion = bf16[384,2048]{1,0:T(8,128)(2,1)} fusion(bf16[769,2048]{1,0:T(8,128)(2,1)} %concatenate.32, s32[1024]{0:T(1024)S(1)} %pad_clamp_fusion.1), kind=kCustom, calls=%fused_computation | custom fusion | bytes 3147264 | tf_op jit(solution)/shard_map/gather | solution.py:163
  76.4 2.4 reshape.420
  78.8 64.7 %all_to_all.21 = bf16[1,32,12,2048]{3,2,0,1:T(8,128)(2,1)S(1)} all-to-all(bf16[1,32,12,2048]{3,2,0,1:T(8,128)(2,1)S(1)} %bitcast.122), channel_id=1, replica_groups=mesh['sp'=32,'tp'=8] {'sp'}, dimensions={1} | all-to-all | bytes 3145728 | tf_op jit(solution)/shard_map/all_to_all | solution.py:164
  143.5 2.0 copy.96
  145.5 0.3 all-gather.6.cloned.1.call-start
  145.8 67.6 %all-gather.4.cloned.1.call-done = bf16[1,32,96,2048]{3,1,0,2:T(8,128)(2,1)} async-done(((bf16[1,32,12,2048]{3,1,0,2:T(8,128)(2,1)}), bf16[1,32,96,2048]{3,1,0,2:T(8,128)(2,1)}) %all-gather.4.cloned.1.call-update) | async-done | bytes 12582928 | tf_op jit(solution)/shard_map/all_gather | solution.py:165
  213.4 11.7 %copy.97 = bf16[1,32,96,2048]{3,2,1,0:T(8,128)(2,1)S(1)} copy(bf16[1,32,96,2048]{3,1,0,2:T(8,128)(2,1)} %all-gather.4.cloned.1.call-done) | data formatting | bytes 25165824 | tf_op jit(solution)/shard_map/all_gather | solution.py:165
  225.2 3.5 fusion.12
  228.7 4.5 %fusion = bf16[3072,128]{1,0:T(8,128)(2,1)} fusion(bf16[3072,2048]{1,0:T(8,128)(2,1)S(1)} %bitcast.121, f32[3072,128]{1,0:T(8,128)S(1)} %fusion.12, bf16[1,2048,128]{2,1,0:T(8,128)(2,1)S(1)} %copy-done.10), kind=kOutput, calls=%fused_computation.8 | convolution fusion | flops 1612972032 | bytes 15466496 | tf_op jit(solution)/shard_map/esd,edf->esf/dot_general | solution.py:170
  233.2 47.5 %all-gather.6.cloned.1.call-done = bf16[3072,1024]{1,0:T(8,128)(2,1)} async-done(((bf16[3072,128]{1,0:T(8,128)(2,1)}), bf16[3072,1024]{1,0:T(8,128)(2,1)}) %all-gather.6.cloned.1.call-update) | async-done | bytes 6291472 | tf_op jit(solution)/shard_map/all_gather | solution.py:176
  280.8 5.7 %convolution_convert_fusion = bf16[3072,256]{1,0:T(8,128)(2,1)} fusion(bf16[3072,1024]{1,0:T(8,128)(2,1)} %all-gather.6.cloned.1.call-done, bf16[1,1024,256]{2,1,0:T(8,128)(2,1)S(1)} %copy-done), kind=kOutput, calls=%fused_computation.6 | convolution fusion | flops 1611399168 | bytes 8388608 | tf_op jit(solution)/shard_map/esf,efc->esc/dot_general | solution.py:174
  286.5 9.9 %all-to-all-start.2 = ((bf16[1,32,96,256]{3,2,0,1:T(8,128)(2,1)}), bf16[1,32,96,256]{3,2,0,1:T(8,128)(2,1)S(1)}, u32[]{:S(2)}, u32[]{:S(2)}) async-start(bf16[1,32,96,256]{3,2,0,1:T(8,128)(2,1)} %bitcast.124), calls=%async_computation.2 | async-start | bytes 3145728 | tf_op jit(solution)/shard_map/all_to_all | solution.py:180
  296.4 0.3 reduce_sum.98
  296.9 0.3 compare_select_fusion
  297.1 0.2 reshape.439
  297.4 0.2 copy.89
  297.6 36.4 %all-to-all-done.2 = bf16[1,32,96,256]{3,2,0,1:T(8,128)(2,1)S(1)} async-done(((bf16[1,32,96,256]{3,2,0,1:T(8,128)(2,1)}), bf16[1,32,96,256]{3,2,0,1:T(8,128)(2,1)S(1)}, u32[]{:S(2)}, u32[]{:S(2)}) %all-to-all-start.2) | async-done | bytes 1572896 | tf_op jit(solution)/shard_map/all_to_all | solution.py:180
  334.0 5.3 %gather_fusion.1 = bf16[1536,256]{1,0:T(8,128)(2,1)} fusion(bf16[3072,256]{1,0:T(8,128)(2,1)S(1)} %bitcast.119, s32[2048]{0:T(1024)S(1)} %pad_clamp_fusion), kind=kCustom, calls=%fused_computation.1 | custom fusion | bytes 1579008 | tf_op jit(solution)/shard_map/gather | solution.py:188
  339.3 2.2 reshape.458
  341.5 4.2 %multiply_reduce_fusion.1 = f32[768,256]{1,0:T(8,128)S(1)} fusion(f32[768,2,256]{2,1,0:T(2,128)S(1)} %reshape.458, f32[768,2]{1,0:T(8,128)S(1)} %copy.89), kind=kLoop, calls=%fused_computation.9 | loop fusion | flops 589824 | bytes 2365440 | tf_op jit(solution)/shard_map/reduce_sum | solution.py:189
  345.7 1.3 fusion.19
  347.1 10.8 %all_to_all.22 = f32[8,1,1536]{2,1,0:T(1,128)S(1)} all-to-all(f32[8,1,1536]{2,1,0:T(1,128)S(1)} %broadcast_in_dim.77), channel_id=1, replica_groups=mesh['sp'=32,'tp'=8] {'tp'}, dimensions={0} | all-to-all | bytes 98304 | tf_op jit(solution)/shard_map/all_to_all | solution.py:32
  357.9 2.0 multiply_convert_fusion.1
  (59 shorter events, 0.7 us)
Async XLA Ops:
  6.5 274.2 %copy-start = (bf16[1,1024,256]{2,1,0:T(8,128)(2,1)S(1)}, bf16[1,1024,256]{2,1,0:T(8,128)(2,1)}, u32[]{:S(2)}) copy-start(bf16[1,1024,256]{2,1,0:T(8,128)(2,1)} %param.28) | copy-start | bytes 1572868
  6.5 18.0 %copy-start.4 = (s32[768]{0:T(1024)S(1)}, s32[768]{0:T(1024)}, u32[]{:S(2)}) copy-start(s32[768]{0:T(1024)} %param.19) | copy-start | bytes 9220
  6.5 18.8 %copy-start.2 = (bf16[768,64]{0,1:T(8,128)(2,1)S(1)}, bf16[768,64]{0,1:T(8,128)(2,1)}, u32[]{:S(2)}) copy-start(bf16[768,64]{0,1:T(8,128)(2,1)} %param.17) | copy-start | bytes 294916
  7.4 17.2 %collective-permute-start.1 = (s32[128]{0:T(128)S(1)}, s32[128]{0:T(128)S(1)}, u32[]{:S(2)}, u32[]{:S(2)}) collective-permute-start(s32[128]{0:T(128)S(1)} %get-tuple-element.16), channel_id=1, source_target_pairs={{0,8},{8,16},{16,24},{24,32},{32,40},{40,48},{48,56},{56,64},{64,7... | collective-permute-start | bytes 1544 | tf_op jit(solution)/shard_map/ppermute | solution.py:22
  11.3 13.3 %collective-permute-start.3 = (s32[128]{0:T(128)S(1)}, s32[128]{0:T(128)S(1)}, u32[]{:S(2)}, u32[]{:S(2)}) collective-permute-start(s32[128]{0:T(128)S(1)} %get-tuple-element.17), channel_id=1, source_target_pairs={{8,0},{16,8},{24,16},{32,24},{40,32},{48,40},{56,48},{64,56},{72,6... | collective-permute-start | bytes 1544 | tf_op jit(solution)/shard_map/ppermute | solution.py:25
  14.4 11.7 %copy-start.7 = (f32[2]{0:T(128)S(1)}, f32[2]{0:T(128)}, u32[]{:S(2)}) copy-start(f32[2]{0:T(128)} %param.20) | copy-start | bytes 28
  14.4 11.3 %collective-permute-start = (bf16[128,128]{0,1:T(8,128)(2,1)S(1)}, bf16[128,128]{0,1:T(8,128)(2,1)S(1)}, u32[]{:S(2)}, u32[]{:S(2)}) collective-permute-start(bf16[128,128]{0,1:T(8,128)(2,1)S(1)} %get-tuple-element.7), channel_id=1, source_target_pairs={{0,8},{8,16},{16,24},{24,32},{32,40},{40,48},{48,56},{56,64},{64,7... | collective-permute-start | bytes 98312 | tf_op jit(solution)/shard_map/ppermute | solution.py:22
  18.4 7.9 %collective-permute-start.2 = (bf16[128,128]{0,1:T(8,128)(2,1)S(1)}, bf16[128,128]{0,1:T(8,128)(2,1)S(1)}, u32[]{:S(2)}, u32[]{:S(2)}) collective-permute-start(bf16[128,128]{0,1:T(8,128)(2,1)S(1)} %get-tuple-element.8), channel_id=1, source_target_pairs={{8,0},{16,8},{24,16},{32,24},{40,32},{48,40},{56,48},{64,56},{72,6... | collective-permute-start | bytes 98312 | tf_op jit(solution)/shard_map/ppermute | solution.py:25
  25.7 1.6 copy-start.3
  29.7 26.6 %all-to-all-start = ((bf16[8,768,128]{1,2,0:T(8,128)(2,1)}), bf16[8,768,128]{1,2,0:T(8,128)(2,1)S(1)}, u32[]{:S(2)}, u32[]{:S(2)}) async-start(bf16[8,768,128]{1,2,0:T(8,128)(2,1)} %broadcast_in_dim.73), calls=%async_computation | async-start | bytes 3145728 | tf_op jit(solution)/shard_map/all_to_all | solution.py:32
  35.7 177.7 %all-gather.4.cloned.1.call-start = ((), (), s32[]{:S(2)}) async-start(), calls=%async_computation.4 | async-start | bytes 14155776 | tf_op jit(solution)/shard_map/all_gather | solution.py:165
  63.7 0.8 copy-start.5
  65.3 1.7 copy-start.1
  145.5 79.6 %copy-start.9 = (bf16[1,2048,128]{2,1,0:T(8,128)(2,1)S(1)}, bf16[1,2048,128]{2,1,0:T(8,128)(2,1)}, u32[]{:S(2)}) copy-start(bf16[1,2048,128]{2,1,0:T(8,128)(2,1)} %param.26) | copy-start | bytes 1572868
  145.5 135.3 %all-gather.6.cloned.1.call-start = ((), (), s32[]{:S(2)}) async-start(), calls=%async_computation.5 | async-start | bytes 7077888 | tf_op jit(solution)/shard_map/all_gather | solution.py:176
  225.1 3.6 copy-start.10
  286.5 10.9 %copy-start.6 = (f32[768,2]{0,1:T(2,128)S(1)}, f32[768,2]{0,1:T(2,128)}, u32[]{:S(2)}) copy-start(f32[768,2]{0,1:T(2,128)} %param.25) | copy-start | bytes 18436
  286.5 47.5 %all-to-all-start.2 = ((bf16[1,32,96,256]{3,2,0,1:T(8,128)(2,1)}), bf16[1,32,96,256]{3,2,0,1:T(8,128)(2,1)S(1)}, u32[]{:S(2)}, u32[]{:S(2)}) async-start(bf16[1,32,96,256]{3,2,0,1:T(8,128)(2,1)} %bitcast.124), calls=%async_computation.2 | async-start | bytes 3145728 | tf_op jit(solution)/shard_map/all_to_all | solution.py:180
  339.3 18.6 %copy-start.8 = (f32[256]{0:T(256)S(1)}, f32[256]{0:T(256)}, u32[]{:S(2)}) copy-start(f32[256]{0:T(256)} %param.29) | copy-start | bytes 3076
Sparse Core Ops, SparseCore 0:
  145.6 67.7 all-gather.3
  233.3 47.3 all-gather.5
where the time goes:
time: 368 us; the launch traced here: 367 us
  waiting for transfers between devices  166 us (45%)
  blocking collectives  75.4 us (20%)
  local copies, waits for them, and re-layouts  44.9 us (12%)
  starting transfers between devices  26.7 us (7%)
  matrix products  23.2 us (6%)
  other arithmetic  17 us (5%)
  between operations  14 us (4%)
    all_gather x1, waiting for transfers between devices, shards(): arrived = lax.all_gather(received, 'tp', axis=2, tiled=True)  67.6 us
    all_to_all x1, blocking collectives, shards(): lax.all_to_all(outgoing, 'sp', split_axis=1, concat_axis=1, tiled=True)  64.7 us
    all_gather x1, waiting for transfers between devices, shards(): lax.all_gather(hidden, 'tp', axis=2, tiled=True)  47.5 us
    all_to_all x1, waiting for transfers between devices, shards(): lax.all_to_all(produced.reshape(experts_local, sp_size, tp_size * capacit...  36.4 us
    all_to_all x1, waiting for transfers between devices, copy_for_each(): return lax.all_to_all(copies, axis, split_axis=0, concat_axis=0, tiled=True)  13.9 us
    all_gather x1, local copies, waits for them, and re-layouts, shards(): arrived = lax.all_gather(received, 'tp', axis=2, tiled=True)  11.7 us
    all_to_all x1, blocking collectives, copy_for_each(): return lax.all_to_all(copies, axis, split_axis=0, concat_axis=0, tiled=True)  10.8 us
    all_to_all x1, starting transfers between devices, shards(): lax.all_to_all(produced.reshape(experts_local, sp_size, tp_size * capacit...  9.93 us
  transfers between devices with their start and end apart: 8, of which 4 were waited for; matrix products, arithmetic and copies ran while one was open for 4% of the time, Pallas kernels for 0%

commit v1 on v0

v1 whole, which is shorter than its diff:
```python
import jax
import jax.numpy as jnp
from jax import lax
from jax.experimental import pallas as pl
from jax.experimental.pallas import tpu as pltpu
from jax.sharding import PartitionSpec as P

HEAD_DIM = 64
HALF = 128
PER_GROUP = 8
ALPHA = 2.0**0.25
EPS = 1e-05
NEG = -1e30
F32 = jnp.float32
BF16 = jnp.bfloat16

ROWS = 768
QB = 128
BLOCKS = ROWS // QB
TP = 8
BLK = ROWS // TP
CAP = 12
MAIN = 8
EXTRA = CAP - MAIN
D = 2048
HALF_D = D // 2
WIDE = D + HALF_D
FF = 1024


def dot(a, b):
    return jnp.dot(a, b, preferred_element_type=F32)


def params(mib=48):
    return pltpu.CompilerParams(vmem_limit_bytes=mib * 1024 * 1024)


def iota(shape, dim):
    return lax.broadcasted_iota(jnp.int32, shape, dim)


def pack_kernel(kt, vt, seg, low, high):
    for out, start, row in ((low, 0, 0), (high, ROWS - HALF, BLOCKS - 1)):
        out[0:64, :] = kt[:, start : start + HALF]
        out[64:128, :] = vt[:, start : start + HALF]
        out[128:144, :] = jnp.broadcast_to(seg[row : row + 1, :].astype(F32), (16, HALF)).astype(BF16)


def attend(q, kt, vt, seg_q, seg_k, sink):
    qs = jnp.concatenate([q[:, :HEAD_DIM], q[:, HEAD_DIM:]], axis=0)
    scores = dot(qs, kt) * HEAD_DIM ** (-0.5)
    col = jnp.transpose(jnp.broadcast_to(seg_q, (QB, QB)))
    row_i = iota((QB, QB), 0)
    col_i = iota((QB, QB), 1)
    parts = []
    for n, band in enumerate((col_i >= row_i, None, col_i <= row_i)):
        same = col == jnp.broadcast_to(seg_k[n], (QB, QB))
        parts.append(same if band is None else jnp.logical_and(same, band))
    allowed = jnp.concatenate(parts, axis=1)
    outs = []
    for h in range(2):
        part = jnp.where(allowed, scores[h * QB : (h + 1) * QB], NEG)
        peak = jnp.maximum(jnp.max(part, -1, keepdims=True), sink[h])
        raised = jnp.where(allowed, jnp.exp(part - peak), 0.0)
        denominator = jnp.sum(raised, -1, keepdims=True) + jnp.exp(sink[h] - peak)
        outs.append((raised / denominator).astype(BF16))
    weights = jnp.concatenate(outs, axis=0)
    got = lax.dot_general(weights, vt, (((1,), (1,)), ((), ())), preferred_element_type=F32)
    return jnp.concatenate([got[:QB], got[QB:]], axis=1).astype(BF16)


def interior_kernel(sink, q, kt, vt, seg, out):
    sinks = [jnp.full((QB, 1), sink[h], F32) for h in range(2)]
    rows = [seg[b : b + 1, :].astype(F32) for b in range(BLOCKS)]
    for b in range(1, BLOCKS - 1):
        lo = (b - 1) * QB
        out[b * QB : (b + 1) * QB, :] = attend(
            q[b * QB : (b + 1) * QB, :],
            kt[:, lo : lo + 3 * QB],
            vt[:, lo : lo + 3 * QB],
            rows[b],
            rows[b - 1 : b + 2],
            sinks,
        )


def edge_kernel(sink, q, kt, vt, seg, before, after, part, out):
    sinks = [jnp.full((QB, 1), sink[h], F32) for h in range(2)]
    rows = [seg[b : b + 1, :].astype(F32) for b in range(BLOCKS)]
    out[QB : ROWS - QB, :] = part[QB : ROWS - QB, :]
    out[:QB, :] = attend(
        q[:QB, :],
        jnp.concatenate([before[0:64, :], kt[:, : 2 * QB]], axis=1),
        jnp.concatenate([before[64:128, :], vt[:, : 2 * QB]], axis=1),
        rows[0],
        [before[128:129, :].astype(F32), rows[0], rows[1]],
        sinks,
    )
    lo = ROWS - QB
    out[lo:, :] = attend(
        q[lo:, :],
        jnp.concatenate([kt[:, lo - QB :], after[0:64, :]], axis=1),
        jnp.concatenate([vt[:, lo - QB :], after[64:128, :]], axis=1),
        rows[BLOCKS - 1],
        [rows[BLOCKS - 2], rows[BLOCKS - 1], after[128:129, :].astype(F32)],
        sinks,
    )


def routing_kernel(ids, weight, rows, cols):
    r0 = iota((BLK, BLK), 0)
    r1 = iota((BLK, BLK), 1)
    eye = r0 == r1

    def column(row):
        return jnp.sum(jnp.where(eye, jnp.broadcast_to(row, (BLK, BLK)), 0.0), axis=1, keepdims=True)

    def place(expert, rank):
        is_main = rank < MAIN - 0.5
        main = jnp.where(is_main, expert * MAIN + rank, -1e6)
        extra = jnp.where(is_main, -1e6, expert * MAIN + (rank - MAIN))
        return main, extra

    id_rows = [ids[k : k + 1, :] for k in range(2)]
    id_cols = [column(row) for row in id_rows]
    row_out, col_out = [], []
    for k in range(2):
        rank_row = jnp.zeros((1, BLK), F32)
        rank_col = jnp.zeros((BLK, 1), F32)
        for other in range(2):
            hit = jnp.logical_and(id_cols[other] == id_rows[k], r0 < r1)
            rank_row += jnp.sum(jnp.where(hit, 1.0, 0.0), axis=0, keepdims=True)
            hit = jnp.logical_and(id_cols[k] == id_rows[other], r1 < r0)
            rank_col += jnp.sum(jnp.where(hit, 1.0, 0.0), axis=1, keepdims=True)
        row_out.append(place(id_rows[k], rank_row))
        col_out.append(place(id_cols[k], rank_col))
    zero_row = jnp.zeros((1, BLK), F32)
    rows[...] = jnp.concatenate(
        [row_out[0][0], row_out[1][0], row_out[0][1], row_out[1][1]] + [zero_row] * 4, axis=0
    )
    lane = iota((BLK, 8), 1)
    table = jnp.zeros((BLK, 8), F32)
    for n, c in enumerate(
        [col_out[0][0], col_out[1][0], col_out[0][1], col_out[1][1]]
        + [column(weight[k : k + 1, :]) for k in range(2)]
    ):
        table = jnp.where(lane == n, c, table)
    cols[...] = table


def project_kernel(place, att, weight, residual, gain, rows, normed_out, sent, acc):
    step = pl.program_id(0)

    @pl.when(step == 0)
    def _():
        acc[...] = ALPHA * residual[...].astype(F32)

    acc[...] += dot(jnp.concatenate([att[0], att[1]], axis=1), weight[...])

    @pl.when(step == pl.num_programs(0) - 1)
    def _():
        summed = acc[...]
        mean_value = jnp.mean(summed, -1, keepdims=True)
        variance = jnp.mean(jnp.square(summed - mean_value), -1, keepdims=True)
        normed = ((summed - mean_value) * lax.rsqrt(variance + EPS) * gain[...]).astype(BF16)
        normed_out[...] = normed
        count = sent.shape[0]
        slot = iota((count, BLK), 0).astype(F32)

        def chosen(first, second, shift):
            hit = jnp.logical_or(
                slot == rows[first : first + 1, :] + shift, slot == rows[second : second + 1, :] + shift
            )
            return jnp.where(hit, 1.0, 0.0).astype(BF16)

        sent[:, :D] = dot(chosen(0, 1, 0.0), normed).astype(BF16)
        sent[:, D:] = (
            dot(chosen(2, 3, 0.0), normed[:, :HALF_D])
            + dot(chosen(2, 3, float(EXTRA)), normed[:, HALF_D:])
        ).astype(BF16)


def expert_kernel(arrived, gate, up, down_low, down_high, out, x, hidden):
    step = pl.program_id(0)
    count = arrived.shape[0]
    extras = count // 2

    def spread(shape, extra_dim, other_dim, shift):
        extra = iota(shape, extra_dim)
        hit = ((extra >> 2) << 3) + (extra & 3) + shift == iota(shape, other_dim)
        return jnp.where(hit, 1.0, 0.0).astype(BF16)

    @pl.when(step == 0)
    def _():
        x[:count, :] = arrived[:, :D]
        for h in range(2):
            x[count:, h * HALF_D : (h + 1) * HALF_D] = dot(
                spread((extras, count), 0, 1, h * EXTRA), arrived[:, D:]
            ).astype(BF16)

    @pl.when(step < 4)
    def _():
        gate_part = dot(x[...], jnp.concatenate([gate[0], gate[1]], axis=1))
        up_part = dot(x[...], jnp.concatenate([up[0], up[1]], axis=1))
        hidden[step] = (jax.nn.silu(gate_part) * up_part).astype(BF16)

    @pl.when(step >= 4)
    def _():
        part = pl.multiple_of((step - 4) * 256, 256)
        extra = jnp.zeros((count, 256), F32)
        for h, down in enumerate((down_low, down_high)):
            got = dot(hidden[0], down[0, 0:256, :])
            for n in range(1, 4):
                got += dot(hidden[n], down[0, n * 256 : (n + 1) * 256, :])
            got = got.astype(BF16)
            out[:, pl.ds(h * HALF_D + part, 256)] = got[:count]
            extra += dot(spread((count, extras), 1, 0, h * EXTRA), got[count:])
        out[:, pl.ds(D + part, 256)] = extra.astype(BF16)


def combine_kernel(returned, normed, cols, out):
    count = returned.shape[0]
    slot = iota((BLK, count), 1).astype(F32)
    combined = [jnp.zeros((BLK, HALF_D), F32) for _ in range(2)]
    for k in range(2):
        main = jnp.where(slot == cols[:, k : k + 1], 1.0, 0.0).astype(BF16)
        weight = cols[:, 4 + k : 5 + k]
        for h in range(2):
            extra = jnp.where(slot == cols[:, 2 + k : 3 + k] + float(h * EXTRA), 1.0, 0.0).astype(BF16)
            got = dot(main, returned[:, h * HALF_D : (h + 1) * HALF_D]) + dot(extra, returned[:, D:])
            combined[h] = combined[h] + weight * got
    summed = ALPHA * normed[...].astype(F32) + jnp.concatenate(combined, axis=1)
    mean_value = jnp.mean(summed, -1, keepdims=True)
    variance = jnp.mean(jnp.square(summed - mean_value), -1, keepdims=True)
    scaled = (summed - mean_value) * lax.rsqrt(variance + EPS)
    width = out.shape[2]
    for n in range(out.shape[0]):
        out[n] = scaled[:, n * width : (n + 1) * width].astype(BF16)


VMEM = pl.BlockSpec(memory_space=pltpu.VMEM)
SMEM = pl.BlockSpec(memory_space=pltpu.SMEM)


def shards(
    residual,
    queries,
    keys,
    values,
    segments,
    sink,
    out_weight,
    norm_gain_one,
    group,
    member,
    route_weight,
    gate_weight,
    up_weight,
    down_weight,
    norm_gain_two,
):
    sp = lax.axis_size("sp")
    place = lax.axis_index("tp")
    gates = lax.all_gather(gate_weight[0], "tp", axis=0)
    ups = lax.all_gather(up_weight[0], "tp", axis=0)
    downs = lax.all_gather(down_weight[0], "tp", axis=0)

    kt = keys.T
    vt = values.T
    seg = (segments + 1).reshape(BLOCKS, QB)
    halo = jax.ShapeDtypeStruct((144, HALF), BF16)
    low, high = pl.pallas_call(
        pack_kernel,
        out_shape=(halo, halo),
        in_specs=[VMEM] * 3,
        out_specs=(VMEM, VMEM),
        compiler_params=params(),
        name="pack",
    )(kt, vt, seg)
    forward = [(i, i + 1) for i in range(sp - 1)]
    before = lax.ppermute(high, "sp", forward)
    after = lax.ppermute(low, "sp", [(t, s) for s, t in forward])

    rows_shape = jax.ShapeDtypeStruct((ROWS, 128), BF16)
    interior = pl.pallas_call(
        interior_kernel,
        out_shape=rows_shape,
        in_specs=[SMEM] + [VMEM] * 4,
        out_specs=VMEM,
        compiler_params=params(),
        name="interior",
    )(sink, queries, kt, vt, seg)

    own = place * BLK
    ids = lax.dynamic_slice(group[None, :] * PER_GROUP + member.T, (0, own), (2, BLK)).astype(F32)
    own_weight = lax.dynamic_slice(route_weight.T, (0, own), (2, BLK))
    rows, cols = pl.pallas_call(
        routing_kernel,
        out_shape=(jax.ShapeDtypeStruct((8, BLK), F32), jax.ShapeDtypeStruct((BLK, 8), F32)),
        in_specs=[VMEM] * 2,
        out_specs=(VMEM, VMEM),
        compiler_params=params(),
        name="routing",
    )(ids, own_weight)

    attended = pl.pallas_call(
        edge_kernel,
        out_shape=rows_shape,
        in_specs=[SMEM] + [VMEM] * 7,
        out_specs=VMEM,
        compiler_params=params(),
        name="edges",
    )(sink, queries, kt, vt, seg, before, after, interior)

    heads = lax.all_to_all(attended.reshape(TP, BLK, 128), "tp", 0, 0, tiled=True)

    slots = sp * MAIN
    normed, sent = pl.pallas_call(
        project_kernel,
        grid_spec=pltpu.PrefetchScalarGridSpec(
            num_scalar_prefetch=1,
            grid=(4,),
            in_specs=[
                pl.BlockSpec((2, BLK, 128), lambda i, p: (i, 0, 0)),
                pl.BlockSpec((256, D), lambda i, p: (i, 0)),
                pl.BlockSpec((BLK, D), lambda i, p: (p[0], 0)),
                pl.BlockSpec((1, D), lambda i, p: (0, 0)),
                pl.BlockSpec((8, BLK), lambda i, p: (0, 0)),
            ],
            out_specs=[
                pl.BlockSpec((BLK, D), lambda i, p: (0, 0)),
                pl.BlockSpec((slots, WIDE), lambda i, p: (0, 0)),
            ],
            scratch_shapes=[pltpu.VMEM((BLK, D), F32)],
        ),
        out_shape=(
            jax.ShapeDtypeStruct((BLK, D), BF16),
            jax.ShapeDtypeStruct((slots, WIDE), BF16),
        ),
        compiler_params=params(),
        name="project",
    )(place.reshape(1), heads, out_weight, residual, norm_gain_one.reshape(1, D), rows)

    arrived = lax.all_to_all(sent.reshape(sp, MAIN, WIDE), "sp", 0, 0, tiled=True)

    produced = pl.pallas_call(
        expert_kernel,
        grid=(8,),
        in_specs=[
            pl.BlockSpec((slots, WIDE), lambda i: (0, 0)),
            pl.BlockSpec((2, D, 128), lambda i: (jnp.minimum(i, 3), 0, 0)),
            pl.BlockSpec((2, D, 128), lambda i: (jnp.minimum(i, 3), 0, 0)),
            pl.BlockSpec((1, FF, 256), lambda i: (jnp.maximum(i - 4, 0), 0, 0)),
            pl.BlockSpec((1, FF, 256), lambda i: (jnp.maximum(i, 4), 0, 0)),
        ],
        out_specs=pl.BlockSpec((slots, WIDE), lambda i: (0, 0)),
        out_shape=jax.ShapeDtypeStruct((slots, WIDE), BF16),
        scratch_shapes=[
            pltpu.VMEM((sp * CAP, D), BF16),
            pltpu.VMEM((4, sp * CAP, 256), BF16),
        ],
        compiler_params=params(),
        name="experts",
    )(arrived.reshape(slots, WIDE), gates, ups, downs, downs)

    returned = lax.all_to_all(produced.reshape(sp, MAIN, WIDE), "sp", 0, 0, tiled=True)

    scaled = pl.pallas_call(
        combine_kernel,
        out_shape=jax.ShapeDtypeStruct((TP, BLK, D // TP), BF16),
        in_specs=[VMEM] * 3,
        out_specs=VMEM,
        compiler_params=params(),
        name="combine",
    )(returned.reshape(slots, WIDE), normed, cols)

    last = lax.all_to_all(scaled, "tp", 0, 0, tiled=True).reshape(ROWS, D // TP)
    return (last.astype(F32) * norm_gain_two).astype(BF16)


def solution(mesh):
    in_specs = (
        P("sp", None),
        P("sp", "tp"),
        P("sp", "tp"),
        P("sp", "tp"),
        P("sp"),
        P("tp"),
        P(),
        P(),
        P("sp"),
        P("sp", None),
        P("sp", None),
        P("sp", None, "tp"),
        P("sp", None, "tp"),
        P("sp", None, "tp"),
        P("tp"),
    )
    out_specs = P("sp", "tp")
    return jax.shard_map(shards, mesh=mesh, in_specs=in_specs, out_specs=out_specs, check_vma=False)
```

time: 368 us -> 205 us (0.56)
  waiting for transfers between devices: 166 us -> 36.2 us
  local copies, waits for them, and re-layouts: 44.9 us -> 6.75 us
  blocking collectives: 75.4 us -> 113 us
  matrix products: 23.2 us -> 0 us
  Pallas kernels: 0 us -> 21.8 us
  starting transfers between devices: 26.7 us -> 10.7 us
  other arithmetic: 17 us -> 3 us
    all_gather x2 -> x3, waiting for transfers between devices: 115 us -> 26.6 us  [the longest x1 26.6 us: shards(): downs = lax.all_gather(down_weight[0], 'tp', axis=0)]
    all_to_all x2 -> x1, waiting for transfers between devices: 50.3 us -> 7.49 us  [shards(): lax.all_to_all(attended.reshape(TP, BLK, 128), 'tp', 0, 0, tiled=True)]
    all_to_all x2 -> x3, blocking collectives: 75.4 us -> 113 us  [the longest x1 51.2 us: shards(): lax.all_to_all(sent.reshape(sp, MAIN, WIDE), 'sp', 0, 0, tiled=True)]
    dot_general x10 -> x0, matrix products: 23.2 us -> none  [the longest x1 7.34 us: shards(): jnp.dot(gather_directly(attended, 'tp', 1), weight_rows, preferred_elemen...]
    pallas_call x0 -> x7, Pallas kernels: none -> 21.8 us  [the longest x1 11.2 us: shards(): pl.pallas_call(expert_kernel, grid=(8,), in_specs=[pl.BlockSpec((slots, W...]
    gather x2 -> x0, local copies, waits for them, and re-layouts: 12.7 us -> none  [the longest x1 7.36 us: shards(): outgoing = extended[source].reshape(experts_local, sp_size, capacity, width)]
    all_gather x1 -> x0, local copies, waits for them, and re-layouts: 11.7 us -> none  [shards(): arrived = lax.all_gather(received, 'tp', axis=2, tiled=True)]
    all_to_all x2 -> x1, starting transfers between devices: 15.9 us -> 5.43 us  [shards(): lax.all_to_all(attended.reshape(TP, BLK, 128), 'tp', 0, 0, tiled=True)]
  transfers between devices with their start and end apart: 8 -> 6, of which waited for: 4 -> 2; matrix products, arithmetic and copies ran while one was open for 4% -> 1% of each run, Pallas kernels for 0% -> 5%
where the time goes in v1:
time: 205 us; the launch traced here: 204 us
  blocking collectives  113 us (55%)
  waiting for transfers between devices  36.2 us (18%)
  Pallas kernels  21.8 us (11%)
  between operations  13.2 us (6%)
  starting transfers between devices  10.7 us (5%)
  local copies, waits for them, and re-layouts  6.75 us (3%)
  other arithmetic  3 us (1%)
    all_to_all x1, blocking collectives, shards(): lax.all_to_all(sent.reshape(sp, MAIN, WIDE), 'sp', 0, 0, tiled=True)  51.2 us
    all_to_all x1, blocking collectives, shards(): lax.all_to_all(produced.reshape(sp, MAIN, WIDE), 'sp', 0, 0, tiled=True)  48.6 us
    all_gather x1, waiting for transfers between devices, shards(): downs = lax.all_gather(down_weight[0], 'tp', axis=0)  26.6 us
    all_to_all x1, blocking collectives, shards(): last = lax.all_to_all(scaled, 'tp', 0, 0, tiled=True).reshape(ROWS, D // TP)  12.8 us
    pallas_call x1, Pallas kernels, shards(): pl.pallas_call(expert_kernel, grid=(8,), in_specs=[pl.BlockSpec((slots, W...  11.2 us
    all_to_all x1, waiting for transfers between devices, shards(): lax.all_to_all(attended.reshape(TP, BLK, 128), 'tp', 0, 0, tiled=True)  7.49 us
    unnamed x24, local copies, waits for them, and re-layouts  6.61 us
    all_to_all x1, starting transfers between devices, shards(): lax.all_to_all(attended.reshape(TP, BLK, 128), 'tp', 0, 0, tiled=True)  5.43 us
  transfers between devices with their start and end apart: 6, of which 2 were waited for; matrix products, arithmetic and copies ran while one was open for 1% of the time, Pallas kernels for 5%

profile of v1, /device:TPU:1, one launch (start us, length us, event | category | flops | bytes accessed | tf_op | source)
XLA Modules:
  0.0 204.3 jit_solution(7364992268538184598)
XLA Ops:
  6.5 0.0 copy-start
  6.5 0.0 copy-start.1
  6.5 0.0 all-gather.4.cloned.1.call-start
  6.5 0.7 all-gather.4.cloned.1.call-update
  7.3 0.0 all-gather.6.cloned.1.call-start
  7.3 0.7 all-gather.6.cloned.1.call-update
  8.0 0.0 all-gather.8.cloned.1.call-start
  8.1 0.7 all-gather.8.cloned.1.call-update
  8.7 0.7 add_bitcast_fusion.seg
  9.4 0.0 copy-start.2
  9.4 0.9 copy-done.2
  10.3 0.0 copy-start.4
  10.3 0.9 copy-done.4
  11.2 3.9 %collective-permute-start = (bf16[144,128]{1,0:T(8,128)(2,1)S(1)}, bf16[144,128]{1,0:T(8,128)(2,1)S(1)}, u32[]{:S(2)}, u32[]{:S(2)}) collective-permute-start(bf16[144,128]{1,0:T(8,128)(2,1)S(1)} %get-tuple-element.11), channel_id=1, source_target_pairs={{0,8},{8,16},{16,24},{24,32},{32,40},{40,48},{48,56},{56,64},{64,7... | collective-permute-start | bytes 110600 | tf_op jit(solution)/shard_map/ppermute | solution.py:282
  15.2 1.3 collective-permute-start.1
  16.5 0.7 broadcast_multiply_fusion
  17.2 0.0 copy-done
  17.2 0.1 dynamic-slice_bitcast_fusion.weight
  17.3 0.1 dynamic-slice.5
  17.3 0.0 copy-start.3
  17.3 0.9 copy-done.3
  18.2 0.0 copy-start.5
  18.2 0.9 copy-done.5
  19.1 0.0 copy-start.6
  19.1 0.9 copy-done.6
  20.0 0.0 copy-start.10
  20.0 0.7 copy-done.10
  20.7 2.4 %interior.1.part = bf16[768,128]{1,0:T(8,128)(2,1)S(1)} custom-call(f32[2]{0:T(128)S(1)} %copy-done.10, bf16[768,128]{1,0:T(8,128)(2,1)S(1)} %copy-done.6, bf16[64,768]{1,0:T(8,128)(2,1)S(1)} %bitcast.23, bf16[64,768]{1,0:T(8,128)(2,1)S(1)} %bitcast.26, s32[6,128]{1,0:T(8,128)S(1)} %add_bitcast_fusion.seg), custom_call_target="tpu_custom_call" | custom-call | tf_op jit(solution)/shard_map/interior/pallas_call | solution.py:286
  23.1 0.0 collective-permute-done.before
  23.1 0.0 collective-permute-done.1.after
  23.1 2.3 %edges.1 = bf16[768,128]{1,0:T(8,128)(2,1)} custom-call(f32[2]{0:T(128)S(1)} %copy-done.10, bf16[768,128]{1,0:T(8,128)(2,1)S(1)} %copy-done.6, bf16[64,768]{1,0:T(8,128)(2,1)S(1)} %bitcast.24, bf16[64,768]{1,0:T(8,128)(2,1)S(1)} %bitcast.27, s32[6,128]{1,0:T(8,128)S(1)} %add_bitcast_fusion.seg, bf16[144,128]{1,0:T(8,128)(2,1)S(1)} %collective-permute-done.before, ...), custom_call_target="tpu_custom_call" | custom-call | tf_op jit(solution)/shard_map/edges/pallas_call | solution.py:307
  25.4 5.4 %all-to-all-start = ((bf16[8,96,128]{2,1,0:T(8,128)(2,1)}), bf16[8,96,128]{2,1,0:T(8,128)(2,1)S(1)}, u32[]{:S(2)}, u32[]{:S(2)}) async-start(bf16[8,96,128]{2,1,0:T(8,128)(2,1)} %bitcast.4), calls=%async_computation | async-start | bytes 393216 | tf_op jit(solution)/shard_map/all_to_all | solution.py:316
  30.8 0.8 fusion.2.ids
  31.6 0.2 routing.1
  31.9 7.5 %all-to-all-done.att = bf16[8,96,128]{2,1,0:T(8,128)(2,1)S(1)} async-done(((bf16[8,96,128]{2,1,0:T(8,128)(2,1)}), bf16[8,96,128]{2,1,0:T(8,128)(2,1)S(1)}, u32[]{:S(2)}, u32[]{:S(2)}) %all-to-all-start) | async-done | bytes 196640 | tf_op jit(solution)/shard_map/all_to_all | solution.py:316
  39.3 0.0 copy-done.1
  39.3 0.0 copy-start.9
  39.3 0.7 copy-done.9
  40.0 4.6 %project.1 = (bf16[96,2048]{1,0:T(8,128)(2,1)S(1)}, bf16[256,3072]{1,0:T(8,128)(2,1)S(1)}) custom-call(s32[1]{0:T(128)} %bitcast.place, bf16[8,96,128]{2,1,0:T(8,128)(2,1)S(1)} %all-to-all-done.att, bf16[1024,2048]{1,0:T(8,128)(2,1)} %weight.1, bf16[768,2048]{1,0:T(8,128)(2,1)S(1)} %copy-done.1, f32[1,2048]{1,0:T(1,128)S(1)} %bitcast.28, ...), custom_call_target="tpu_custom_call" | custom-call | tf_op jit(solution)/shard_map/project/pallas_call | solution.py:319
  44.6 0.0 copy-start.7
  44.6 0.7 copy-done.7
  45.4 51.2 %all_to_all.20 = bf16[32,8,3072]{2,1,0:T(8,128)(2,1)S(1)} all-to-all(bf16[32,8,3072]{2,1,0:T(8,128)(2,1)S(1)} %bitcast.21), channel_id=1, replica_groups=mesh['sp'=32,'tp'=8] {'sp'}, dimensions={0} | all-to-all | bytes 3145728 | tf_op jit(solution)/shard_map/all_to_all | solution.py:345
  96.5 0.0 all-gather.4.cloned.1.call-done.gate
  96.5 0.0 all-gather.6.cloned.1.call-done.up
  96.5 26.6 %all-gather.8.cloned.1.call-done.down_low.down_high = bf16[8,1024,256]{2,1,0:T(8,128)(2,1)} async-done(((bf16[1,1024,256]{2,1,0:T(8,128)(2,1)}), bf16[8,1024,256]{2,1,0:T(8,128)(2,1)}) %all-gather.8.cloned.1.call-update) | async-done | bytes 4194320 | tf_op jit(solution)/shard_map/all_gather | solution.py:267
  123.2 11.2 %experts.1 = bf16[256,3072]{1,0:T(8,128)(2,1)S(1)} custom-call(bf16[256,3072]{1,0:T(8,128)(2,1)S(1)} %bitcast.18, bf16[8,2048,128]{2,1,0:T(8,128)(2,1)} %all-gather.4.cloned.1.call-done.gate, bf16[8,2048,128]{2,1,0:T(8,128)(2,1)} %all-gather.6.cloned.1.call-done.up, bf16[8,1024,256]{2,1,0:T(8,128)(2,1)} %all-gather.8.cloned.1.call-done.down_low.down_high, ...), custom_call_target="tpu_custom_call" | custom-call | tf_op jit(solution)/shard_map/experts/pallas_call | solution.py:347
  134.4 0.0 copy-start.8
  134.4 0.0 copy-start.11
  134.4 48.6 %all_to_all.21 = bf16[32,8,3072]{2,1,0:T(8,128)(2,1)S(1)} all-to-all(bf16[32,8,3072]{2,1,0:T(8,128)(2,1)S(1)} %bitcast.20), channel_id=1, replica_groups=mesh['sp'=32,'tp'=8] {'sp'}, dimensions={0} | all-to-all | bytes 3145728 | tf_op jit(solution)/shard_map/all_to_all | solution.py:367
  183.0 0.0 copy-done.8
  183.0 1.1 combine.1
  184.2 12.8 %all_to_all.22 = bf16[8,96,256]{2,1,0:T(8,128)(2,1)S(1)} all-to-all(bf16[8,96,256]{2,1,0:T(8,128)(2,1)S(1)} %combine.1), channel_id=1, replica_groups=mesh['sp'=32,'tp'=8] {'tp'}, dimensions={0} | all-to-all | bytes 786432 | tf_op jit(solution)/shard_map/all_to_all | solution.py:378
  196.9 0.0 copy-done.11
  196.9 0.8 fusion
  (1 shorter events, 0.0 us)
Async XLA Ops:
  6.5 10.6 %copy-start = (f32[768,2]{0,1:T(2,128)S(1)}, f32[768,2]{0,1:T(2,128)}, u32[]{:S(2)}) copy-start(f32[768,2]{0,1:T(2,128)} %param.25) | copy-start | bytes 18436
  6.5 32.8 %copy-start.1 = (bf16[768,2048]{1,0:T(8,128)(2,1)S(1)}, bf16[768,2048]{1,0:T(8,128)(2,1)}, u32[]{:S(2)}) copy-start(bf16[768,2048]{1,0:T(8,128)(2,1)} %residual.1) | copy-start | bytes 9437188
  6.5 90.0 %all-gather.4.cloned.1.call-start = ((), (), s32[]{:S(2)}) async-start(), calls=%async_computation.4 | async-start | bytes 4718592 | tf_op jit(solution)/shard_map/all_gather | solution.py:265
  7.3 89.2 %all-gather.6.cloned.1.call-start = ((), (), s32[]{:S(2)}) async-start(), calls=%async_computation.5 | async-start | bytes 4718592 | tf_op jit(solution)/shard_map/all_gather | solution.py:266
  8.0 115.1 %all-gather.8.cloned.1.call-start = ((), (), s32[]{:S(2)}) async-start(), calls=%async_computation.6 | async-start | bytes 4718592 | tf_op jit(solution)/shard_map/all_gather | solution.py:267
  9.4 0.9 copy-start.2
  10.3 0.9 copy-start.4
  11.2 11.9 %collective-permute-start = (bf16[144,128]{1,0:T(8,128)(2,1)S(1)}, bf16[144,128]{1,0:T(8,128)(2,1)S(1)}, u32[]{:S(2)}, u32[]{:S(2)}) collective-permute-start(bf16[144,128]{1,0:T(8,128)(2,1)S(1)} %get-tuple-element.11), channel_id=1, source_target_pairs={{0,8},{8,16},{16,24},{24,32},{32,40},{40,48},{48,56},{56,64},{64,7... | collective-permute-start | bytes 110600 | tf_op jit(solution)/shard_map/ppermute | solution.py:282
  15.2 7.9 %collective-permute-start.1 = (bf16[144,128]{1,0:T(8,128)(2,1)S(1)}, bf16[144,128]{1,0:T(8,128)(2,1)S(1)}, u32[]{:S(2)}, u32[]{:S(2)}) collective-permute-start(bf16[144,128]{1,0:T(8,128)(2,1)S(1)} %get-tuple-element.12), channel_id=1, source_target_pairs={{8,0},{16,8},{24,16},{32,24},{40,32},{48,40},{56,48},{64,56},{72,6... | collective-permute-start | bytes 110600 | tf_op jit(solution)/shard_map/ppermute | solution.py:283
  17.3 0.9 copy-start.3
  18.2 0.9 copy-start.5
  19.1 0.9 copy-start.6
  20.0 0.7 copy-start.10
  25.4 13.9 %all-to-all-start = ((bf16[8,96,128]{2,1,0:T(8,128)(2,1)}), bf16[8,96,128]{2,1,0:T(8,128)(2,1)S(1)}, u32[]{:S(2)}, u32[]{:S(2)}) async-start(bf16[8,96,128]{2,1,0:T(8,128)(2,1)} %bitcast.4), calls=%async_computation | async-start | bytes 393216 | tf_op jit(solution)/shard_map/all_to_all | solution.py:316
  39.3 0.7 copy-start.9
  44.6 0.7 copy-start.7
  134.4 48.7 %copy-start.8 = (bf16[96,2048]{1,0:T(8,128)(2,1)S(1)}, bf16[96,2048]{1,0:T(8,128)(2,1)}, u32[]{:S(2)}) copy-start(bf16[96,2048]{1,0:T(8,128)(2,1)} %copy-done.7) | copy-start | bytes 1179652
  134.4 62.5 %copy-start.11 = (f32[256]{0:T(256)S(1)}, f32[256]{0:T(256)}, u32[]{:S(2)}) copy-start(f32[256]{0:T(256)} %param.29) | copy-start | bytes 3076
Sparse Core Ops, SparseCore 0:
  9.2 40.9 all-gather.3
  52.0 34.5 all-gather.5
  88.5 34.5 all-gather.7
